TPU v7x, 32 devices: a whole 2x2x4 slice. The times are simulated.
32 devices in a mesh: sp: 8 (over z, y), tp: 4 (over x, core).
Axes of the slice: x: 2, y: 2, z: 4, core: 2. Of those that a mesh axis runs over, the one named last changes fastest.
Arguments:
- queries: bfloat16 [8192, 1024], P('sp', 'tp'), may hold values from -6 to 6
- keys: bfloat16 [8192, 1024], P('sp', 'tp'), may hold values from -6 to 6
- values: bfloat16 [8192, 1024], P('sp', 'tp'), may hold values from -6 to 6
- gates: bfloat16 [8192, 1024], P('sp', 'tp'), may hold values from -6 to 6
- log_decay: float32 [8192, 8], P('sp', 'tp'), may hold values from -1.6 to 0, as said below
- norm_gain: float32 [8, 128], P('tp'), may hold values from 0.1 to 1.9
- out_weight: bfloat16 [1024, 2048], P('tp'), may hold values from -0.1875 to 0.1875
- resid: bfloat16 [8192, 2048], P(('sp', 'tp')), may hold values from -6 to 6
- post_mix_gain: float32 [2048], replicated, may hold values from 0.1 to 1.9
- pre_ffn_gain: float32 [2048], replicated, may hold values from 0.1 to 1.9
- w_gate: bfloat16 [2048, 5632], P('sp', 'tp'), may hold values from -0.125 to 0.125
- w_up: bfloat16 [2048, 5632], P('sp', 'tp'), may hold values from -0.125 to 0.125
- w_down: bfloat16 [5632, 2048], P('tp', 'sp'), may hold values from -0.078125 to 0.078125
- post_ffn_gain: float32 [2048], replicated, may hold values from 0.1 to 1.9
Outputs:
- updated: bfloat16 [8192, 2048], P(('sp', 'tp'))
Inputs may be any that keep to these rules, and one draw needn't show every extreme that they name: `log_decay`: every entry is negative.
All inputs are finite; a program needn't handle non-finite values.
Results may differ from a plain program's by a relative error of at most 0.02.
Values may be sent and summed in bfloat16 or wider, within the bound.
A program may use at most 128 MiB of HBM per device.

v0:
```python
import jax
import jax.numpy as jnp
from jax import lax
from jax.sharding import PartitionSpec as P

BLOCK = 512
EPSILON = 1e-06


def entering(x, axis, join, neutral):
    place = lax.axis_index(axis)
    gathered = jax.tree.map(
        lambda a, kind: lax.all_gather(a.astype(kind), axis), x, (jnp.bfloat16, jnp.bfloat16)
    )
    state = jax.tree.map(lambda a, e: jnp.zeros_like(a) + jnp.asarray(e, a.dtype), x, neutral)

    def one(step, state):
        return join(
            state,
            jax.tree.map(
                lambda a, own: lax.dynamic_index_in_dim(a, step, 0, False).astype(own.dtype),
                gathered,
                x,
            ),
        )

    return lax.fori_loop(0, place, one, state)


def rms_norm(values_in, gain_vec):
    widened = values_in.astype(jnp.float32)
    return (
        widened
        * lax.rsqrt(jnp.mean(widened * widened, axis=-1, keepdims=True) + EPSILON)
        * gain_vec
    )


def block_step(carried, pieces):
    query_blk, key_blk, value_blk, decay_blk = pieces
    length = query_blk.shape[1]
    key_scale = query_blk.shape[2] ** (-0.5)
    cumulative = jnp.cumsum(decay_blk, axis=1)
    log_gap = cumulative[:, :, None] - cumulative[:, None, :]
    causal = lax.broadcasted_iota(jnp.int32, (length, length), 0) >= lax.broadcasted_iota(
        jnp.int32, (length, length), 1
    )
    weight = jnp.where(causal[None], jnp.exp(jnp.minimum(log_gap, 0.0)), 0.0)
    products = jnp.einsum("htd,hsd->hts", query_blk, key_blk, preferred_element_type=jnp.float32)
    scores = (products * key_scale * weight).astype(jnp.bfloat16)
    within = jnp.einsum("hts,hsd->htd", scores, value_blk, preferred_element_type=jnp.float32)
    carried_term = (
        jnp.einsum(
            "htd,hde->hte", query_blk.astype(jnp.float32), carried, precision=lax.Precision.HIGHEST
        )
        * jnp.exp(cumulative)[:, :, None]
    )
    to_end = jnp.exp(cumulative[:, -1:] - cumulative) * key_scale
    scaled_keys = (key_blk.astype(jnp.float32) * to_end[:, :, None]).astype(jnp.bfloat16)
    added = jnp.einsum("hsd,hse->hde", scaled_keys, value_blk, preferred_element_type=jnp.float32)
    carried = jnp.exp(cumulative[:, -1])[:, None, None] * carried + added
    return (carried, within + carried_term)


def to_blocks(matrix, block_len, head_count):
    row_count = matrix.shape[0]
    return matrix.reshape(row_count // block_len, block_len, head_count, -1).transpose(0, 2, 1, 3)


def finish_heads(retention, gates, norm_gain):
    centered = retention - jnp.mean(retention, axis=-1, keepdims=True)
    variance = jnp.mean(centered * centered, axis=-1, keepdims=True)
    normed = centered * lax.rsqrt(variance + EPSILON) * norm_gain[None]
    gate_vals = gates.astype(jnp.float32).reshape(normed.shape)
    return (jax.nn.silu(gate_vals) * normed).reshape(normed.shape[0], -1).astype(jnp.bfloat16)


def combine_states(earlier, later):
    return (earlier[0] * later[0], later[0][:, None, None] * earlier[1] + later[1])


def per_device(
    queries,
    keys,
    values,
    gates,
    log_decay,
    norm_gain,
    out_weight,
    resid,
    post_mix_gain,
    pre_ffn_gain,
    w_gate,
    w_up,
    w_down,
    post_ffn_gain,
):
    row_count = queries.shape[0]
    head_count = log_decay.shape[1]
    head_dim = queries.shape[1] // head_count
    block_count = row_count // BLOCK
    query_blocks = to_blocks(queries, BLOCK, head_count)
    key_blocks = to_blocks(keys, BLOCK, head_count)
    value_blocks = to_blocks(values, BLOCK, head_count)
    decay_blocks = log_decay.reshape(block_count, BLOCK, head_count).transpose(0, 2, 1)
    start_state = jnp.zeros((head_count, head_dim, head_dim), jnp.float32)
    local_state, outputs = lax.scan(
        block_step, start_state, (query_blocks, key_blocks, value_blocks, decay_blocks)
    )
    retention = outputs.transpose(0, 2, 1, 3).reshape(row_count, head_count, head_dim)
    cumulative = jnp.cumsum(log_decay, axis=0)
    local_decay = jnp.exp(cumulative[-1])
    identity = (jnp.ones_like(local_decay), jnp.zeros_like(local_state))
    incoming = entering((local_decay, local_state), "sp", combine_states, identity)
    query_rows = queries.reshape(row_count, head_count, head_dim).astype(jnp.float32)
    retention = (
        retention
        + jnp.einsum("thd,hde->the", query_rows, incoming[1], precision=lax.Precision.HIGHEST)
        * jnp.exp(cumulative)[:, :, None]
    )
    retained = finish_heads(retention, gates, norm_gain)
    quarter = resid.shape[0]
    regrouped = lax.all_to_all(retained, "tp", split_axis=0, concat_axis=1, tiled=True)
    group_rows = out_weight.shape[0]
    empty_mix = jnp.zeros((quarter, out_weight.shape[1]), jnp.float32)
    running = empty_mix
    shard_piece = lax.all_gather(out_weight, "tp", axis=0, tiled=True)
    for offset in range(shard_piece.shape[0] // group_rows):
        columns = lax.dynamic_slice_in_dim(regrouped, offset * group_rows, group_rows, 1)
        part = jnp.dot(
            columns,
            shard_piece[offset * group_rows : (offset + 1) * group_rows],
            preferred_element_type=jnp.float32,
        )
        running = running + part.astype(jnp.bfloat16).astype(jnp.float32)
    mixed = running
    mixed = mixed.astype(jnp.bfloat16)
    middle = (resid.astype(jnp.float32) + rms_norm(mixed, post_mix_gain)).astype(jnp.bfloat16)
    ffn_input = rms_norm(middle, pre_ffn_gain).astype(jnp.bfloat16)
    gathered = lax.all_gather(ffn_input, "tp", axis=0, tiled=True)
    columns = gathered
    gate_act = jnp.dot(
        columns,
        lax.all_gather(w_gate, "sp", axis=0, tiled=True),
        preferred_element_type=jnp.float32,
    )
    up_act = jnp.dot(
        columns, lax.all_gather(w_up, "sp", axis=0, tiled=True), preferred_element_type=jnp.float32
    )
    down_full = lax.all_gather(w_down, "sp", axis=1, tiled=True)
    hidden = (jax.nn.silu(gate_act) * up_act).astype(jnp.bfloat16)
    branch = lax.psum_scatter(
        jnp.dot(hidden, down_full, preferred_element_type=jnp.float32)
        .astype(jnp.bfloat16)
        .astype(jnp.float32)
        .astype(jnp.bfloat16),
        "tp",
        scatter_dimension=0,
        tiled=True,
    )
    return (middle.astype(jnp.float32) + rms_norm(branch, post_ffn_gain)).astype(jnp.bfloat16)


def solution(mesh):
    in_specs = (
        P("sp", "tp"),
        P("sp", "tp"),
        P("sp", "tp"),
        P("sp", "tp"),
        P("sp", "tp"),
        P("tp", None),
        P("tp", None),
        P(("sp", "tp"), None),
        P(),
        P(),
        P("sp", "tp"),
        P("sp", "tp"),
        P("tp", "sp"),
        P(),
    )
    out_specs = P(("sp", "tp"), None)
    return jax.shard_map(
        per_device, mesh=mesh, in_specs=in_specs, out_specs=out_specs, check_vma=False
    )
```

profile of v0, /device:TPU:0, one launch (start us, length us, event | category | flops | bytes accessed | tf_op | source)
XLA Modules:
  0.0 438.4 jit_solution(6785753459974340258)
XLA Ops:
  6.5 0.7 all-gather.8.cloned.1.call-update
  7.3 0.7 all-gather.12.cloned.1.call-update
  8.1 0.7 copy.104
  8.8 0.6 reduce-window.16
  9.4 0.2 slice_reduce_fusion.1
  9.5 0.2 reduce-window.17
  9.7 0.1 add_bitcast_fusion.1
  9.8 0.2 fusion.48
  10.0 22.3 %all-gather.1 = bf16[8,1,2]{2,1,0:T(2,128)(2,1)S(1)} all-gather(bf16[1,1,2]{2,1,0:T(2,128)(2,1)S(1)} %bitcast.154), channel_id=1, replica_groups=mesh['sp'=8,'tp'=4] {'sp'}, dimensions={0}, use_global_device_ids=true | all-gather | bytes 36 | tf_op jit(solution)/shard_map/all_gather | solution.py:13
  32.3 0.1 copy.58
  32.4 0.1 reshape.172
  32.5 0.1 reshape.173
  32.7 0.1 reshape.174
  32.8 9.6 %while.26 = (s32[]{:T(128)}, f32[2,128,128]{2,1,0:T(8,128)S(1)}, f32[2,2,512,128]{3,2,1,0:T(8,128)}, f32[2,2,512]{2,1,0:T(2,128)S(1)}, bf16[2,2,512,128]{3,1,2,0...) while((s32[]{:T(128)}, f32[2,128,128]{2,1,0:T(8,128)S(1)}, ...), condition=%wide.region_3.4_spmd.clone, body=%wide.region_0.3_spmd.clone.sunk | while | flops 507643936 | bytes 5702508 | solution.py:107
  32.8 0.6 reduce-window.26
  33.5 0.2 slice_reduce_fusion.3
  33.6 0.2 reduce-window.27
  33.9 0.4 constant_dynamic-slice_fusion.12
  34.3 0.2 constant_dynamic-slice_fusion.11
  34.4 0.1 iota_compare_fusion.2
  34.5 1.0 fusion.75
  35.7 0.1 copy.124
  35.8 0.1 fusion.74
  35.8 1.2 fusion.76
  37.0 0.5 convolution_add_fusion.2
  37.6 0.6 reduce-window.26
  38.2 0.2 slice_reduce_fusion.3
  38.4 0.2 reduce-window.27
  38.7 0.4 constant_dynamic-slice_fusion.12
  39.0 0.2 constant_dynamic-slice_fusion.11
  39.2 0.1 iota_compare_fusion.2
  39.3 1.0 fusion.75
  40.4 0.1 copy.124
  40.5 0.1 fusion.74
  40.6 1.2 fusion.76
  41.8 0.5 convolution_add_fusion.2
  42.4 1.6 copy.57
  44.1 0.9 reshape.175
  45.0 0.2 copy.53
  45.2 33.1 %all-gather = bf16[16,128,128]{2,1,0:T(8,128)(2,1)S(1)} all-gather(bf16[2,128,128]{2,1,0:T(8,128)(2,1)S(1)} %convert_element_type.103), channel_id=2, replica_groups=mesh['sp'=8,'tp'=4] {'sp'}, dimensions={0}, use_global_device_ids=true | all-gather | bytes 589824 | tf_op jit(solution)/shard_map/all_gather | solution.py:13
  78.4 0.7 fusion.51
  79.1 0.1 multiply_reduce_fusion
  79.3 0.4 multiply_convert_fusion.4
  79.7 0.4 convert_element_type.105
  80.1 11.4 %all_to_all.16 = bf16[4,256,256]{1,2,0:T(8,128)(2,1)S(1)} all-to-all(bf16[4,256,256]{1,2,0:T(8,128)(2,1)S(1)} %copy.62), channel_id=1, replica_groups=mesh['sp'=8,'tp'=4] {'tp'}, dimensions={0} | all-to-all | bytes 1048576 | tf_op jit(solution)/shard_map/all_to_all | solution.py:123
  91.5 1.8 fusion.22
  93.4 1.7 fusion.23
  95.1 0.5 fusion.24
  95.6 0.8 fusion.25
  96.4 0.4 copy-done.3
  96.8 0.6 fusion.31
  97.4 1.3 fusion.33
  98.8 0.5 all-gather.14.cloned.1.call-update
  99.4 0.5 all-gather.16.cloned.1.call-update
  99.9 0.2 reduce-scatter.2.cloned.1.call-start
  100.1 41.9 %all-gather.12.cloned.1.call-done = bf16[2048,1408]{1,0:T(8,128)(2,1)} async-done(((bf16[256,1408]{1,0:T(8,128)(2,1)}), bf16[2048,1408]{1,0:T(8,128)(2,1)}) %all-gather.12.cloned.1.call-update) | async-done | bytes 5767184 | tf_op jit(solution)/shard_map/all_gather | solution.py:144
  142.0 34.2 %all-gather.10.cloned.1.call-done = bf16[1024,2048]{1,0:T(8,128)(2,1)} async-done(((bf16[256,2048]{1,0:T(8,128)(2,1)}), bf16[1024,2048]{1,0:T(8,128)(2,1)}) %all-gather.10.cloned.1.call-update) | async-done | bytes 4194320 | tf_op jit(solution)/shard_map/all_gather | solution.py:140
  176.3 11.7 %fusion.52 = f32[1024,1408]{1,0:T(8,128)} fusion(bf16[1024,2048]{1,0:T(8,128)(2,1)} %all-gather.10.cloned.1.call-done, bf16[2048,1408]{1,0:T(8,128)(2,1)} %all-gather.12.cloned.1.call-done), kind=kOutput, calls=%fused_computation.97 | convolution fusion | flops 5905580032 | bytes 15728640 | tf_op jit(solution)/shard_map/dot_general | solution.py:142
  188.0 82.7 %all-gather.14.cloned.1.call-done = bf16[2048,1408]{1,0:T(8,128)(2,1)} async-done(((bf16[256,1408]{1,0:T(8,128)(2,1)}), bf16[2048,1408]{1,0:T(8,128)(2,1)}) %all-gather.14.cloned.1.call-update) | async-done | bytes 5767184 | tf_op jit(solution)/shard_map/all_gather | solution.py:148
  270.7 93.2 %all-gather.16.cloned.1.call-done = bf16[1408,2048]{1,0:T(8,128)(2,1)} async-done(((bf16[1408,256]{1,0:T(8,128)(2,1)}), bf16[1408,2048]{1,0:T(8,128)(2,1)}) %all-gather.16.cloned.1.call-update) | async-done | bytes 5767184 | tf_op jit(solution)/shard_map/all_gather | solution.py:150
  363.9 20.5 %convolution_convert_fusion = bf16[1024,2048]{1,0:T(8,128)(2,1)} fusion(bf16[1408,2048]{1,0:T(8,128)(2,1)} %all-gather.16.cloned.1.call-done, f32[1024,1408]{1,0:T(8,128)} %fusion.52, bf16[1024,2048]{1,0:T(8,128)(2,1)} %all-gather.10.cloned.1.call-done, bf16[2048,1408]{1,0:T(8,128)(2,1)} %all-gather.14.cloned.1.call-done), kind=kOutput, calls=%fused_computation.38 | convolution fusion | flops 11821907968 | bytes 25690112 | tf_op jit(solution)/shard_map/dot_general | solution.py:153
  384.5 42.9 %reduce-scatter.2.cloned.1.call-done = bf16[256,2048]{1,0:T(8,128)(2,1)} async-done(((bf16[1024,2048]{1,0:T(8,128)(2,1)}), bf16[256,2048]{1,0:T(8,128)(2,1)}) %reduce-scatter.2.cloned.1.call-update) | async-done | bytes 1048592 | tf_op jit(solution)/shard_map/reduce_scatter | solution.py:152
  427.4 1.5 fusion.29
  428.9 2.6 fusion.34
  (56 shorter events, 0.8 us)
Async XLA Ops:
  6.5 25.8 %copy-start.5 = (bf16[1024,256]{1,0:T(8,128)(2,1)S(1)}, bf16[1024,256]{1,0:T(8,128)(2,1)}, u32[]{:S(2)}) copy-start(bf16[1024,256]{1,0:T(8,128)(2,1)} %param.19) | copy-start | bytes 1572868
  6.5 26.0 %copy-start.6 = (bf16[1024,256]{1,0:T(8,128)(2,1)S(1)}, bf16[1024,256]{1,0:T(8,128)(2,1)}, u32[]{:S(2)}) copy-start(bf16[1024,256]{1,0:T(8,128)(2,1)} %param.20) | copy-start | bytes 1572868
  6.5 26.1 %copy-start.1 = (bf16[1024,256]{1,0:T(8,128)(2,1)S(1)}, bf16[1024,256]{1,0:T(8,128)(2,1)}, u32[]{:S(2)}) copy-start(bf16[1024,256]{1,0:T(8,128)(2,1)} %param.18) | copy-start | bytes 1572868
  6.5 85.0 %all-gather.8.cloned.1.call-start = ((), (), s32[]{:S(2)}) async-start(), calls=%async_computation.2 | async-start | bytes 5242880 | tf_op jit(solution)/shard_map/all_gather | solution.py:127
  7.3 25.5 %copy-start.7 = (f32[1024,2]{0,1:T(2,128)S(1)}, f32[1024,2]{0,1:T(2,128)}, u32[]{:S(2)}) copy-start(f32[1024,2]{0,1:T(2,128)} %param.22) | copy-start | bytes 24580
  7.3 134.8 %all-gather.12.cloned.1.call-start = ((), (), s32[]{:S(2)}) async-start(), calls=%async_computation.4 | async-start | bytes 6488064 | tf_op jit(solution)/shard_map/all_gather | solution.py:144
  8.0 168.3 %all-gather.10.cloned.1.call-start = ((), (), s32[]{:S(2)}) async-start(), calls=%async_computation.3 | async-start | bytes 5242880 | tf_op jit(solution)/shard_map/all_gather | solution.py:140
  42.4 2.6 copy-start.4
  45.0 33.4 %copy-start.2 = (bf16[1024,256]{1,0:T(8,128)(2,1)S(1)}, bf16[1024,256]{1,0:T(8,128)(2,1)}, u32[]{:S(2)}) copy-start(bf16[1024,256]{1,0:T(8,128)(2,1)} %param.18) | copy-start | bytes 1572868
  78.3 0.9 copy-start.11
  91.5 3.5 copy-start
  95.5 1.2 copy-start.3
  95.5 1.2 copy-start.8
  96.4 1.1 copy-start.9
  98.7 171.9 %all-gather.14.cloned.1.call-start = ((), (), s32[]{:S(2)}) async-start(), calls=%async_computation.5 | async-start | bytes 6488064 | tf_op jit(solution)/shard_map/all_gather | solution.py:148
  99.3 264.6 %all-gather.16.cloned.1.call-start = ((), (), s32[]{:S(2)}) async-start(), calls=%async_computation.6 | async-start | bytes 6488064 | tf_op jit(solution)/shard_map/all_gather | solution.py:150
  99.9 327.5 %reduce-scatter.2.cloned.1.call-start = ((), (), s32[]{:S(2)}) async-start(), calls=%async_computation.7 | async-start | bytes 5242880 | tf_op jit(solution)/shard_map/reduce_scatter | solution.py:152
  384.4 44.5 %copy-start.10 = (f32[2048]{0:T(1024)S(1)}, f32[2048]{0:T(1024)}, u32[]{:S(2)}) copy-start(f32[2048]{0:T(1024)} %param.31) | copy-start | bytes 24580
Sparse Core Ops, SparseCore 0:
  8.9 37.1 all-gather.7
  48.3 93.7 all-gather.11
  143.6 32.6 all-gather.9
  178.3 92.3 all-gather.13
  272.6 91.2 all-gather.15
  384.6 42.7 reduce-scatter.1
where the time goes:
time: 439 us; the launch traced here: 438 us
  waiting for transfers between devices  297 us (68%)
  blocking collectives  66.8 us (15%)
  matrix products  43.3 us (10%)
  between operations  13.8 us (3%)
  other arithmetic  9.76 us (2%)
  local copies, waits for them, and re-layouts  6.82 us (2%)
    all_gather x1, waiting for transfers between devices, per_device(): down_full = lax.all_gather(w_down, 'sp', axis=1, tiled=True)  93.2 us
    all_gather x1, waiting for transfers between devices, per_device(): lax.all_gather(w_up, 'sp', axis=0, tiled=True)  82.7 us
    all_gather x2, blocking collectives, entering(): lax.all_gather(a.astype(kind), axis)  55.4 us
    reduce_scatter x1, waiting for transfers between devices, per_device(): lax.psum_scatter(jnp.dot(hidden, down_full, preferred_element_type=jnp.fl...  42.9 us
    all_gather x1, waiting for transfers between devices, per_device(): lax.all_gather(w_gate, 'sp', axis=0, tiled=True)  41.9 us
    all_gather x1, waiting for transfers between devices, per_device(): gathered = lax.all_gather(ffn_input, 'tp', axis=0, tiled=True)  34.2 us
    dot_general x1, matrix products, per_device(): jnp.dot(hidden, down_full, preferred_element_type=jnp.float32)  20.5 us
    dot_general x1, matrix products, per_device(): jnp.dot(columns, lax.all_gather(w_gate, 'sp', axis=0, tiled=True), prefer...  11.7 us
  transfers between devices with their start and end apart: 6, of which 5 were waited for; matrix products, arithmetic and copies ran while one was open for 8% of the time, Pallas kernels for 0%

commit v1 on v0

--- a/solution.py
+++ b/solution.py
@@ -5,6 +5,18 @@
 
 BLOCK = 512
 EPSILON = 1e-06
+
+
+def attach_the_task(mine, across):
+    return jnp.concatenate(
+        jax.lax.all_to_all(
+            jnp.stack(jax.lax.psum(1, across) * [mine]),
+            axis_name=across,
+            split_axis=0,
+            concat_axis=0,
+        ),
+        axis=0,
+    )
 
 
 def entering(x, axis, join, neutral):
@@ -144,9 +156,7 @@
         lax.all_gather(w_gate, "sp", axis=0, tiled=True),
         preferred_element_type=jnp.float32,
     )
-    up_act = jnp.dot(
-        columns, lax.all_gather(w_up, "sp", axis=0, tiled=True), preferred_element_type=jnp.float32
-    )
+    up_act = jnp.dot(columns, attach_the_task(w_up, "sp"), preferred_element_type=jnp.float32)
     down_full = lax.all_gather(w_down, "sp", axis=1, tiled=True)
     hidden = (jax.nn.silu(gate_act) * up_act).astype(jnp.bfloat16)
     branch = lax.psum_scatter(

time: 439 us -> 418 us (0.952)
  waiting for transfers between devices: 297 us -> 269 us
  starting transfers between devices: 0.38 us -> 5.04 us
    all_gather x1 -> x0, waiting for transfers between devices: 82.7 us -> none  [per_device(): lax.all_gather(w_up, 'sp', axis=0, tiled=True)]
    all_gather x1, waiting for transfers between devices: 41.9 us -> 77.9 us  [per_device(): lax.all_gather(w_gate, 'sp', axis=0, tiled=True)]
    all_gather x1, waiting for transfers between devices: 34.2 us -> 63.2 us  [per_device(): gathered = lax.all_gather(ffn_input, 'tp', axis=0, tiled=True)]
    all_gather x1, waiting for transfers between devices: 93.2 us -> 76.3 us  [per_device(): down_full = lax.all_gather(w_down, 'sp', axis=1, tiled=True)]
    all_to_all x0 -> x1, waiting for transfers between devices: none -> 7.07 us  [attach_the_task(): jax.lax.all_to_all(jnp.stack(jax.lax.psum(1, across) * [mine]), axis_name...]
    all_to_all x0 -> x1, starting transfers between devices: none -> 4.7 us  [attach_the_task(): jax.lax.all_to_all(jnp.stack(jax.lax.psum(1, across) * [mine]), axis_name...]
  transfers between devices with their start and end apart: 6 -> 6, of which waited for: 5 -> 5; matrix products, arithmetic and copies ran while one was open for 8% -> 9% of each run, Pallas kernels for 0% -> 0%
where the time goes in v1:
time: 418 us; the launch traced here: 417 us
  waiting for transfers between devices  269 us (64%)
  blocking collectives  66.8 us (16%)
  matrix products  43.2 us (10%)
  between operations  13.5 us (3%)
  local copies, waits for them, and re-layouts  9.79 us (2%)
  other arithmetic  9.75 us (2%)
  starting transfers between devices  5.04 us (1%)
    all_gather x1, waiting for transfers between devices, per_device(): lax.all_gather(w_gate, 'sp', axis=0, tiled=True)  77.9 us
    all_gather x1, waiting for transfers between devices, per_device(): down_full = lax.all_gather(w_down, 'sp', axis=1, tiled=True)  76.3 us
    all_gather x1, waiting for transfers between devices, per_device(): gathered = lax.all_gather(ffn_input, 'tp', axis=0, tiled=True)  63.2 us
    all_gather x2, blocking collectives, entering(): lax.all_gather(a.astype(kind), axis)  55.4 us
    reduce_scatter x1, waiting for transfers between devices, per_device(): lax.psum_scatter(jnp.dot(hidden, down_full, preferred_element_type=jnp.fl...  42.9 us
    dot_general x1, matrix products, per_device(): jnp.dot(hidden, down_full, preferred_element_type=jnp.float32)  20.5 us
    dot_general x1, matrix products, per_device(): jnp.dot(columns, lax.all_gather(w_gate, 'sp', axis=0, tiled=True), prefer...  11.7 us
    all_to_all x1, blocking collectives, per_device(): lax.all_to_all(retained, 'tp', split_axis=0, concat_axis=1, tiled=True)  11.4 us
  transfers between devices with their start and end apart: 6, of which 5 were waited for; matrix products, arithmetic and copies ran while one was open for 9% of the time, Pallas kernels for 0%

profile of v1, /device:TPU:0, one launch (start us, length us, event | category | flops | bytes accessed | tf_op | source)
XLA Modules:
  0.0 417.5 jit_solution(11709244750776716072)
XLA Ops:
  6.5 0.7 all-gather.7.cloned.1.call-update
  7.3 0.7 all-gather.11.cloned.1.call-update
  8.1 0.7 copy.104
  8.8 0.6 reduce-window.16
  9.4 0.2 slice_reduce_fusion.1
  9.5 0.2 reduce-window.17
  9.8 0.2 fusion.48
  10.0 22.3 %all-gather.1 = bf16[8,1,2]{2,1,0:T(2,128)(2,1)S(1)} all-gather(bf16[1,1,2]{2,1,0:T(2,128)(2,1)S(1)} %bitcast.155), channel_id=1, replica_groups=mesh['sp'=8,'tp'=4] {'sp'}, dimensions={0}, use_global_device_ids=true | all-gather | bytes 36 | tf_op jit(solution)/shard_map/all_gather | solution.py:25
  32.3 0.1 copy.58
  32.4 0.1 reshape.177
  32.5 0.1 reshape.178
  32.7 0.1 reshape.179
  32.8 9.5 %while.26 = (s32[]{:T(128)}, f32[2,128,128]{2,1,0:T(8,128)S(1)}, f32[2,2,512,128]{3,2,1,0:T(8,128)}, f32[2,2,512]{2,1,0:T(2,128)S(1)}, bf16[2,2,512,128]{3,1,2,0...) while((s32[]{:T(128)}, f32[2,128,128]{2,1,0:T(8,128)S(1)}, ...), condition=%wide.region_3.4_spmd.clone, body=%wide.region_0.3_spmd.clone.sunk | while | flops 507643936 | bytes 5702508 | solution.py:119
  32.8 0.6 reduce-window.26
  33.5 0.2 slice_reduce_fusion.3
  33.6 0.2 reduce-window.27
  33.9 0.4 constant_dynamic-slice_fusion.12
  34.2 0.2 constant_dynamic-slice_fusion.11
  34.4 0.1 iota_compare_fusion.2
  34.5 1.0 fusion.75
  35.6 0.1 copy.124
  35.7 0.1 fusion.74
  35.8 1.2 fusion.76
  37.0 0.5 convolution_add_fusion.2
  37.6 0.6 reduce-window.26
  38.2 0.2 slice_reduce_fusion.3
  38.4 0.2 reduce-window.27
  38.6 0.4 constant_dynamic-slice_fusion.12
  39.0 0.2 constant_dynamic-slice_fusion.11
  39.2 0.1 iota_compare_fusion.2
  39.3 1.0 fusion.75
  40.4 0.1 copy.124
  40.5 0.1 fusion.74
  40.6 1.2 fusion.76
  41.7 0.5 convolution_add_fusion.2
  42.3 1.7 copy.57
  44.0 0.9 reshape.180
  44.9 0.2 copy.53
  45.1 33.1 %all-gather = bf16[16,128,128]{2,1,0:T(8,128)(2,1)S(1)} all-gather(bf16[2,128,128]{2,1,0:T(8,128)(2,1)S(1)} %convert_element_type.103), channel_id=2, replica_groups=mesh['sp'=8,'tp'=4] {'sp'}, dimensions={0}, use_global_device_ids=true | all-gather | bytes 589824 | tf_op jit(solution)/shard_map/all_gather | solution.py:25
  78.3 0.7 fusion.51
  79.0 0.1 multiply_reduce_fusion
  79.2 0.4 multiply_convert_fusion.4
  79.6 0.4 convert_element_type.105
  80.0 11.4 %all_to_all.21 = bf16[4,256,256]{1,2,0:T(8,128)(2,1)S(1)} all-to-all(bf16[4,256,256]{1,2,0:T(8,128)(2,1)S(1)} %copy.62), channel_id=1, replica_groups=mesh['sp'=8,'tp'=4] {'tp'}, dimensions={0} | all-to-all | bytes 1048576 | tf_op jit(solution)/shard_map/all_to_all | solution.py:135
  91.4 1.8 fusion.22
  93.3 1.7 fusion.23
  95.0 0.5 fusion.24
  95.5 0.8 fusion.25
  96.3 0.4 copy-done.3
  96.7 0.6 fusion.31
  97.3 1.3 fusion.33
  98.7 2.9 stack.2
  101.6 4.7 %all-to-all-start.1 = ((bf16[8,256,1408]{2,1,0:T(8,128)(2,1)}), bf16[8,256,1408]{2,1,0:T(8,128)(2,1)}, u32[]{:S(2)}, u32[]{:S(2)}) async-start(bf16[8,256,1408]{2,1,0:T(8,128)(2,1)} %stack.2), calls=%async_computation.1 | async-start | bytes 11534336 | tf_op jit(solution)/shard_map/all_to_all | solution.py:12
  106.4 0.5 all-gather.13.cloned.1.call-update
  106.9 0.2 reduce-scatter.2.cloned.1.call-start
  107.1 77.9 %all-gather.11.cloned.1.call-done = bf16[2048,1408]{1,0:T(8,128)(2,1)} async-done(((bf16[256,1408]{1,0:T(8,128)(2,1)}), bf16[2048,1408]{1,0:T(8,128)(2,1)}) %all-gather.11.cloned.1.call-update) | async-done | bytes 5767184 | tf_op jit(solution)/shard_map/all_gather | solution.py:156
  185.0 63.2 %all-gather.9.cloned.1.call-done = bf16[1024,2048]{1,0:T(8,128)(2,1)} async-done(((bf16[256,2048]{1,0:T(8,128)(2,1)}), bf16[1024,2048]{1,0:T(8,128)(2,1)}) %all-gather.9.cloned.1.call-update) | async-done | bytes 4194320 | tf_op jit(solution)/shard_map/all_gather | solution.py:152
  248.2 11.7 %fusion.52 = f32[1024,1408]{1,0:T(8,128)} fusion(bf16[1024,2048]{1,0:T(8,128)(2,1)} %all-gather.9.cloned.1.call-done, bf16[2048,1408]{1,0:T(8,128)(2,1)} %all-gather.11.cloned.1.call-done), kind=kOutput, calls=%fused_computation.97 | convolution fusion | flops 5905580032 | bytes 15728640 | tf_op jit(solution)/shard_map/dot_general | solution.py:154
  260.0 7.1 %all-to-all-done.1 = bf16[8,256,1408]{2,1,0:T(8,128)(2,1)} async-done(((bf16[8,256,1408]{2,1,0:T(8,128)(2,1)}), bf16[8,256,1408]{2,1,0:T(8,128)(2,1)}, u32[]{:S(2)}, u32[]{:S(2)}) %all-to-all-start.1) | async-done | bytes 5767200 | tf_op jit(solution)/shard_map/all_to_all | solution.py:12
  267.0 76.3 %all-gather.13.cloned.1.call-done = bf16[1408,2048]{1,0:T(8,128)(2,1)} async-done(((bf16[1408,256]{1,0:T(8,128)(2,1)}), bf16[1408,2048]{1,0:T(8,128)(2,1)}) %all-gather.13.cloned.1.call-update) | async-done | bytes 5767184 | tf_op jit(solution)/shard_map/all_gather | solution.py:160
  343.3 20.5 %convolution_convert_fusion = bf16[1024,2048]{1,0:T(8,128)(2,1)} fusion(bf16[1408,2048]{1,0:T(8,128)(2,1)} %all-gather.13.cloned.1.call-done, f32[1024,1408]{1,0:T(8,128)} %fusion.52, bf16[1024,2048]{1,0:T(8,128)(2,1)} %all-gather.9.cloned.1.call-done, bf16[2048,1408]{1,0:T(8,128)(2,1)} %bitcast.17), kind=kOutput, calls=%fused_computation.38 | convolution fusion | flops 11821907968 | bytes 25690112 | tf_op jit(solution)/shard_map/dot_general | solution.py:163
  363.9 42.9 %reduce-scatter.2.cloned.1.call-done = bf16[256,2048]{1,0:T(8,128)(2,1)} async-done(((bf16[1024,2048]{1,0:T(8,128)(2,1)}), bf16[256,2048]{1,0:T(8,128)(2,1)}) %reduce-scatter.2.cloned.1.call-update) | async-done | bytes 1048592 | tf_op jit(solution)/shard_map/reduce_scatter | solution.py:162
  406.8 1.5 fusion.29
  408.3 2.6 fusion.34
  (58 shorter events, 0.8 us)
Async XLA Ops:
  6.5 25.8 %copy-start.6 = (bf16[1024,256]{1,0:T(8,128)(2,1)S(1)}, bf16[1024,256]{1,0:T(8,128)(2,1)}, u32[]{:S(2)}) copy-start(bf16[1024,256]{1,0:T(8,128)(2,1)} %param.19) | copy-start | bytes 1572868
  6.5 26.0 %copy-start.7 = (bf16[1024,256]{1,0:T(8,128)(2,1)S(1)}, bf16[1024,256]{1,0:T(8,128)(2,1)}, u32[]{:S(2)}) copy-start(bf16[1024,256]{1,0:T(8,128)(2,1)} %param.20) | copy-start | bytes 1572868
  6.5 26.1 %copy-start.1 = (bf16[1024,256]{1,0:T(8,128)(2,1)S(1)}, bf16[1024,256]{1,0:T(8,128)(2,1)}, u32[]{:S(2)}) copy-start(bf16[1024,256]{1,0:T(8,128)(2,1)} %param.18) | copy-start | bytes 1572868
  6.5 84.9 %all-gather.7.cloned.1.call-start = ((), (), s32[]{:S(2)}) async-start(), calls=%async_computation.3 | async-start | bytes 5242880 | tf_op jit(solution)/shard_map/all_gather | solution.py:139
  7.3 25.5 %copy-start.8 = (f32[1024,2]{0,1:T(2,128)S(1)}, f32[1024,2]{0,1:T(2,128)}, u32[]{:S(2)}) copy-start(f32[1024,2]{0,1:T(2,128)} %param.22) | copy-start | bytes 24580
  7.3 177.7 %all-gather.11.cloned.1.call-start = ((), (), s32[]{:S(2)}) async-start(), calls=%async_computation.5 | async-start | bytes 6488064 | tf_op jit(solution)/shard_map/all_gather | solution.py:156
  8.0 240.2 %all-gather.9.cloned.1.call-start = ((), (), s32[]{:S(2)}) async-start(), calls=%async_computation.4 | async-start | bytes 5242880 | tf_op jit(solution)/shard_map/all_gather | solution.py:152
  42.3 2.6 copy-start.5
  44.9 33.4 %copy-start.2 = (bf16[1024,256]{1,0:T(8,128)(2,1)S(1)}, bf16[1024,256]{1,0:T(8,128)(2,1)}, u32[]{:S(2)}) copy-start(bf16[1024,256]{1,0:T(8,128)(2,1)} %param.18) | copy-start | bytes 1572868
  78.3 0.9 copy-start.12
  91.4 3.5 copy-start
  95.4 1.2 copy-start.3
  95.4 1.2 copy-start.9
  96.2 1.1 copy-start.10
  97.3 1.3 copy-start.4
  101.6 165.4 %all-to-all-start.1 = ((bf16[8,256,1408]{2,1,0:T(8,128)(2,1)}), bf16[8,256,1408]{2,1,0:T(8,128)(2,1)}, u32[]{:S(2)}, u32[]{:S(2)}) async-start(bf16[8,256,1408]{2,1,0:T(8,128)(2,1)} %stack.2), calls=%async_computation.1 | async-start | bytes 11534336 | tf_op jit(solution)/shard_map/all_to_all | solution.py:12
  106.3 237.0 %all-gather.13.cloned.1.call-start = ((), (), s32[]{:S(2)}) async-start(), calls=%async_computation.6 | async-start | bytes 6488064 | tf_op jit(solution)/shard_map/all_gather | solution.py:160
  106.9 299.9 %reduce-scatter.2.cloned.1.call-start = ((), (), s32[]{:S(2)}) async-start(), calls=%async_computation.7 | async-start | bytes 5242880 | tf_op jit(solution)/shard_map/reduce_scatter | solution.py:162
  363.8 44.5 %copy-start.11 = (f32[2048]{0:T(1024)S(1)}, f32[2048]{0:T(1024)}, u32[]{:S(2)}) copy-start(f32[2048]{0:T(1024)} %param.31) | copy-start | bytes 24580
Sparse Core Ops, SparseCore 0:
  8.9 37.1 all-gather.6
  48.3 136.6 all-gather.10
  186.6 61.6 all-gather.8
  250.1 93.1 all-gather.12
  364.0 42.7 reduce-scatter.1
